TPU v7x, 32 devices: a whole 2x2x4 slice. The times are simulated.
32 devices in a mesh: grp: 2 (over y), sp: 4 (over z), tp: 4 (over x, core).
Axes of the slice: x: 2, y: 2, z: 4, core: 2. Of those that a mesh axis runs over, the one named last changes fastest.
Arguments:
- queries: bfloat16 [2048, 2048], P(('grp', 'sp'), 'tp'), parts along dimension 0, may hold values from -6 to 6
- keys: bfloat16 [2048, 512], P(('grp', 'sp'), 'tp'), parts along dimension 0, may hold values from -6 to 6
- values: bfloat16 [2048, 512], P(('grp', 'sp'), 'tp'), parts along dimension 0, may hold values from -6 to 6
- query_gain: float32 [128], replicated, may hold values from 1 to 5, as said below
- key_norm_gain: float32 [128], replicated, may hold values from 1 to 5, as said below
- out_weight: bfloat16 [2048, 2048], P('tp'), may hold values from -0.125 to 0.125
- residual: bfloat16 [2048, 2048], P(('grp', 'sp')), parts along dimension 0, may hold values from -0.59765625 to 0.59765625
- mixer_gain: float32 [2048], replicated, may hold values from 0.1 to 1.9
- gate_weight: bfloat16 [2048, 5632], P('sp', 'tp'), may hold values from -0.125 to 0.125
- up_weight: bfloat16 [2048, 5632], P('sp', 'tp'), may hold values from -0.125 to 0.125
- conv_taps: float32 [3, 5632], P(None, 'tp'), may hold values from -3.5 to 3.5
- down_weight: bfloat16 [5632, 2048], P('tp', 'sp'), may hold values from -0.078125 to 0.078125
Outputs:
- layer_out: bfloat16 [2048, 2048], P(('grp', 'sp', 'tp')), parts along dimension 0
There are 2 independent parts, one for each index of `grp`. A program takes and returns all parts, laid end to end along the dimension named above; an argument that names none is the same for every part. Nothing has to cross between parts.
Inputs may be any that keep to these rules, and one draw needn't show every extreme that they name: `query_gain`: positive. `key_norm_gain`: positive.
All inputs are finite; a program needn't handle non-finite values.
Results may differ from a plain program's by a relative error of at most 0.024.
Values may be sent and summed in bfloat16 or wider, within the bound.
A program may use at most 128 MiB of HBM per device.

v0:
```python
import math
import jax
import jax.numpy as jnp
from jax import lax
from jax.sharding import PartitionSpec as P

GRID = 64
norm_eps = 1e-06
rope_base = 10000.0


def padded_2(block, sides, width):
    for axis, dim in sides:
        count = lax.axis_size(axis)
        forward = [(i, i + 1) for i in range(count - 1)]
        backward = [(target, source) for source, target in forward]
        low = lax.ppermute(
            lax.slice_in_dim(block, block.shape[dim] - width, None, axis=dim), axis, forward
        )
        high = lax.ppermute(lax.slice_in_dim(block, 0, width, axis=dim), axis, backward)
        block = jnp.concatenate([low, block, high], axis=dim)
    return block


def angle_tables(positions, head_dim):
    quarter = head_dim // 4
    freqs = 1.0 / rope_base ** (jnp.arange(quarter, dtype=jnp.float32) * 4.0 / head_dim)
    grid_row = (positions // GRID).astype(jnp.float32)
    grid_col = (positions % GRID).astype(jnp.float32)
    by_row = grid_row[:, None] * freqs[None, :]
    by_col = grid_col[:, None] * freqs[None, :]
    angles = jnp.concatenate([by_row, by_row, by_col, by_col], axis=-1)
    return (jnp.cos(angles), jnp.sin(angles))


def apply_rotary(field, cosine_table, sine_table):
    half = field.shape[-1] // 2
    quarter = half // 2
    first = field[..., :half]
    second = field[..., half:]
    turned = jnp.concatenate(
        [
            -first[..., quarter:],
            first[..., :quarter],
            -second[..., quarter:],
            second[..., :quarter],
        ],
        axis=-1,
    )
    return field * cosine_table[:, None, :] + turned * sine_table[:, None, :]


def per_head_norm(field, gain):
    floats = field.astype(jnp.float32)
    return floats * lax.rsqrt(jnp.mean(floats * floats, axis=-1, keepdims=True) + norm_eps) * gain


def local(
    queries,
    keys,
    values,
    query_gain,
    key_norm_gain,
    out_weight,
    residual,
    mixer_gain,
    gate_weight,
    up_weight,
    conv_taps,
    down_weight,
):
    tok_rows = queries.shape[0]
    head_dim = query_gain.shape[0]
    heads_here = queries.shape[1] // head_dim
    kv_here = keys.shape[1] // head_dim
    query_group = heads_here // kv_here
    part_rows = tok_rows // lax.axis_size("tp")
    positions = lax.axis_index("sp") * tok_rows + jnp.arange(tok_rows, dtype=jnp.int32)
    cosine_table, sine_table = angle_tables(positions, head_dim)
    rotated_queries = apply_rotary(
        per_head_norm(queries.reshape(tok_rows, heads_here, head_dim), query_gain),
        cosine_table,
        sine_table,
    ).astype(jnp.bfloat16)
    rotated_keys = apply_rotary(
        per_head_norm(keys.reshape(tok_rows, kv_here, head_dim), key_norm_gain),
        cosine_table,
        sine_table,
    ).astype(jnp.bfloat16)
    key_flat = rotated_keys.reshape(tok_rows, kv_here * head_dim)
    query_mat = jnp.transpose(
        rotated_queries.reshape(tok_rows, kv_here, query_group, head_dim), (1, 2, 0, 3)
    )
    query_mat = query_mat.reshape(kv_here, query_group * tok_rows, head_dim)
    scale = head_dim ** (-0.5)
    start_state = (
        jnp.full((kv_here, query_group * tok_rows), -jnp.inf, jnp.float32),
        jnp.zeros((kv_here, query_group * tok_rows), jnp.float32),
        jnp.zeros((kv_here, query_group * tok_rows, head_dim), jnp.float32),
    )
    key_piece = lax.all_gather(key_flat, "sp", axis=0, tiled=True)
    value_piece = lax.all_gather(values, "sp", axis=0, tiled=True)
    piece_rows = key_piece.shape[0]
    block_slice = math.gcd(piece_rows, 512)
    key_blocks = key_piece.reshape(piece_rows // block_slice, block_slice, kv_here, head_dim)
    value_blocks = value_piece.reshape(piece_rows // block_slice, block_slice, kv_here, head_dim)

    def one_block(state, block_pair):
        running, totals, accum = state
        key_block, value_block = block_pair
        scores = (
            jnp.einsum("hqd,khd->hqk", query_mat, key_block, preferred_element_type=jnp.float32)
            * scale
        )
        new_max = jnp.maximum(running, jnp.max(scores, axis=-1))
        factor = jnp.exp(running - new_max)
        expo = jnp.exp(scores - new_max[..., None])
        totals = totals * factor + jnp.sum(expo, axis=-1)
        accum = accum * factor[..., None] + jnp.einsum(
            "hqk,khd->hqd",
            expo.astype(jnp.bfloat16),
            value_block,
            preferred_element_type=jnp.float32,
        )
        return ((new_max, totals, accum), None)

    result, unused = lax.scan(one_block, start_state, (key_blocks, value_blocks))
    running, totals, accum = result
    heads = (accum / totals[..., None]).astype(jnp.bfloat16)
    heads = jnp.transpose(heads.reshape(kv_here, query_group, tok_rows, head_dim), (2, 0, 1, 3))
    heads = heads.reshape(tok_rows, heads_here * head_dim)
    own_start = lax.axis_index("tp") * part_rows
    full_proj = lax.psum(
        jnp.dot(heads, out_weight, preferred_element_type=jnp.float32).astype(jnp.bfloat16), "tp"
    ).astype(jnp.float32)
    mixed = residual.astype(jnp.float32) + full_proj
    normed = per_head_norm(mixed, mixer_gain).astype(jnp.bfloat16)
    mixed_keep = lax.dynamic_slice_in_dim(mixed, own_start, part_rows, 0)
    gate_acc = jnp.dot(
        normed,
        lax.all_gather(gate_weight, "sp", axis=0, tiled=True),
        preferred_element_type=jnp.float32,
    )
    up_acc = jnp.dot(
        normed,
        lax.all_gather(up_weight, "sp", axis=0, tiled=True),
        preferred_element_type=jnp.float32,
    )
    gate = gate_acc.astype(jnp.bfloat16)
    up_val = up_acc.astype(jnp.bfloat16)
    padded = padded_2(gate, (("sp", 0),), 1).astype(jnp.float32)
    conv = conv_taps[0] * padded[:-2] + conv_taps[1] * padded[1:-1] + conv_taps[2] * padded[2:]
    hidden = (jax.nn.silu(conv) * up_val.astype(jnp.float32)).astype(jnp.bfloat16)
    down_full = lax.all_gather(down_weight, "sp", axis=1, tiled=True)
    mixer_out = lax.psum_scatter(
        jnp.dot(hidden, down_full, preferred_element_type=jnp.float32).astype(jnp.bfloat16),
        "tp",
        scatter_dimension=0,
        tiled=True,
    ).astype(jnp.float32)
    return (mixed_keep + mixer_out).astype(jnp.bfloat16)


def solution(mesh):
    in_specs = (
        P(("grp", "sp"), "tp"),
        P(("grp", "sp"), "tp"),
        P(("grp", "sp"), "tp"),
        P(),
        P(),
        P("tp", None),
        P(("grp", "sp"), None),
        P(),
        P("sp", "tp"),
        P("sp", "tp"),
        P(None, "tp"),
        P("tp", "sp"),
    )
    out_specs = P(("grp", "sp", "tp"), None)
    return jax.shard_map(local, mesh=mesh, in_specs=in_specs, out_specs=out_specs, check_vma=False)
```

profile of v0, /device:TPU:0, one launch (start us, length us, event | category | flops | bytes accessed | tf_op | source)
XLA Modules:
  0.0 424.0 jit_solution(16997622798966750573)
XLA Ops:
  7.4 0.0 copy-start
  7.4 0.0 all-reduce.2.cloned.1.call-start
  7.4 1.3 reshape.324
  8.7 1.9 reshape.323
  10.6 1.0 fusion.32
  11.5 0.9 fusion.34
  12.5 0.2 fusion.39
  12.7 0.3 multiply_reduce_fusion.2
  13.0 0.0 copy-done.7
  13.1 0.3 multiply_multiply_fusion
  13.4 0.0 copy-start.3
  13.4 0.0 copy-start.6
  13.4 0.0 copy-start.2
  13.4 0.9 fusion.28
  14.3 0.1 broadcast_multiply_fusion.1
  14.5 0.0 copy-done.3
  14.5 0.0 copy-done.6
  14.5 0.6 fusion.37
  15.1 0.0 copy-start.4
  15.1 0.0 copy-done.2
  15.2 1.2 fusion.31
  16.4 15.7 %all_gather.15 = bf16[1024,128]{1,0:T(8,128)(2,1)S(1)} all-gather(bf16[256,128]{1,0:T(8,128)(2,1)S(1)} %get-tuple-element.109), channel_id=1, replica_groups=mesh['grp'=2,'sp'=4,'tp'=4] {'sp'}, dimensions={0}, use_global_device_ids=true | all-gather | bytes 327680 | tf_op jit(solution)/shard_map/all_gather | solution.py:101
  32.0 0.0 copy-done.4
  32.0 14.6 %all_gather.16 = bf16[1024,128]{1,0:T(8,128)(2,1)S(1)} all-gather(bf16[256,128]{1,0:T(8,128)(2,1)S(1)} %copy-done.4), channel_id=1, replica_groups=mesh['grp'=2,'sp'=4,'tp'=4] {'sp'}, dimensions={0}, use_global_device_ids=true | all-gather | bytes 327680 | tf_op jit(solution)/shard_map/all_gather | solution.py:102
  46.6 9.3 %while.15 = (s32[]{:T(128)}, f32[1,1024]{1,0:T(1,128)S(1)}, f32[1,1024]{1,0:T(1,128)S(1)}, f32[1,1024,128]{2,1,0:T(8,128)S(1)}, bf16[2,512,1,128]{3,1,2,0:T(8,12...) while((s32[]{:T(128)}, f32[1,1024]{1,0:T(1,128)S(1)}, ...), condition=%wide.region_5.6_spmd.clone, body=%wide.region_2.5_spmd.clone.sunk | while | flops 273028096 | bytes 16318605 | solution.py:127
  46.6 1.8 multiply_reduce_fusion.4
  48.4 2.1 fusion.63
  50.5 0.1 copy-done.1
  50.6 0.6 fusion.65
  51.3 1.8 multiply_reduce_fusion.4
  53.1 2.1 fusion.63
  55.2 0.1 copy-done.1
  55.3 0.6 fusion.65
  55.9 0.2 divide_convert_fusion
  56.1 0.1 copy.27
  56.3 0.0 copy-done
  56.3 1.7 convolution_convert_fusion
  58.0 0.0 all-reduce.2.cloned.1.call-update
  58.0 0.0 all-gather.4.cloned.1.call-start
  58.1 0.5 all-gather.4.cloned.1.call-update
  58.6 0.0 all-gather.6.cloned.1.call-start
  58.7 0.5 all-gather.6.cloned.1.call-update
  59.2 0.0 all-gather.8.cloned.1.call-start
  59.2 0.5 all-gather.8.cloned.1.call-update
  59.8 0.0 copy-start.8
  59.8 0.0 reduce-scatter.2.cloned.1.call-start
  59.8 35.8 %all-reduce.2.cloned.1.call-done = bf16[256,2048]{1,0:T(8,128)(2,1)} async-done(((bf16[256,2048]{1,0:T(8,128)(2,1)}), bf16[256,2048]{1,0:T(8,128)(2,1)}) %all-reduce.2.cloned.1.call-update) | async-done | bytes 1048592 | tf_op jit(solution)/shard_map/psum | solution.py:133
  95.7 3.2 convert_add_fusion
  98.9 68.7 %all-gather.4.cloned.1.call-done = bf16[2048,1408]{1,0:T(8,128)(2,1)} async-done(((bf16[512,1408]{1,0:T(8,128)(2,1)}), bf16[2048,1408]{1,0:T(8,128)(2,1)}) %all-gather.4.cloned.1.call-update) | async-done | bytes 5767184 | tf_op jit(solution)/shard_map/all_gather | solution.py:141
  167.6 0.0 copy-done.8
  167.6 5.1 %convolution_convert_fusion.2 = bf16[256,1408]{1,0:T(8,128)(2,1)S(1)} fusion(bf16[2048,1408]{1,0:T(8,128)(2,1)} %all-gather.4.cloned.1.call-done, f32[2048]{0:T(1024)S(1)} %copy-done.8, f32[256]{0:T(256)S(1)} %add_rsqrt_fusion.1, bf16[256,2048]{1,0:T(8,128)(2,1)} %all-reduce.2.cloned.1.call-done, bf16[256,2048]{1,0:T(8,128)(2,1)} %param.20), kind=kOutput, calls=%fused_computation.29 | convolution fusion | flops 1479901184 | bytes 8594432 | tf_op jit(solution)/shard_map/dot_general | solution.py:139
  172.8 1.3 collective-permute-start
  174.1 1.5 collective-permute-start.1
  175.6 0.0 copy-done.5
  175.6 0.1 slice_reduce_fusion.2
  175.6 0.0 collective-permute-done
  175.6 4.0 collective-permute-done.1
  179.6 1.3 maximum_convert_fusion
  180.9 93.1 %all-gather.6.cloned.1.call-done = bf16[2048,1408]{1,0:T(8,128)(2,1)} async-done(((bf16[512,1408]{1,0:T(8,128)(2,1)}), bf16[2048,1408]{1,0:T(8,128)(2,1)}) %all-gather.6.cloned.1.call-update) | async-done | bytes 5767184 | tf_op jit(solution)/shard_map/all_gather | solution.py:146
  274.0 106.2 %all-gather.8.cloned.1.call-done = bf16[1408,2048]{1,0:T(8,128)(2,1)} async-done(((bf16[1408,512]{1,0:T(8,128)(2,1)}), bf16[1408,2048]{1,0:T(8,128)(2,1)}) %all-gather.8.cloned.1.call-update) | async-done | bytes 5767184 | tf_op jit(solution)/shard_map/all_gather | solution.py:154
  380.2 11.1 %convolution_convert_fusion.3 = bf16[256,2048]{1,0:T(8,128)(2,1)} fusion(bf16[1408,2048]{1,0:T(8,128)(2,1)} %all-gather.8.cloned.1.call-done, bf16[2048,1408]{1,0:T(8,128)(2,1)} %all-gather.6.cloned.1.call-done, f32[258,1408]{1,0:T(8,128)} %maximum_convert_fusion, f32[1408]{0:T(1024)S(1)} %get-tuple-element.91, f32[1408]{0:T(1024)S(1)} %get-tuple-element.92, ...), kind=kOutput, calls=%fused_computation.30 | convolution fusion | flops 2961145856 | bytes 19031552 | tf_op jit(solution)/shard_map/dot_general | solution.py:156
  391.3 0.0 reduce-scatter.2.cloned.1.call-update
  391.3 23.2 %reduce-scatter.2.cloned.1.call-done = bf16[64,2048]{1,0:T(8,128)(2,1)} async-done(((bf16[256,2048]{1,0:T(8,128)(2,1)}), bf16[64,2048]{1,0:T(8,128)(2,1)}) %reduce-scatter.2.cloned.1.call-update) | async-done | bytes 262160 | tf_op jit(solution)/shard_map/reduce_scatter | solution.py:155
  414.5 1.9 add_convert_fusion
  (20 shorter events, 0.2 us)
Async XLA Ops:
  7.4 48.9 %copy-start = (bf16[512,2048]{1,0:T(8,128)(2,1)S(1)}, bf16[512,2048]{1,0:T(8,128)(2,1)}, u32[]{:S(2)}) copy-start(bf16[512,2048]{1,0:T(8,128)(2,1)} %param.19) | copy-start | bytes 6291460
  7.4 5.7 %copy-start.7 = (f32[128]{0:T(128)S(1)}, f32[128]{0:T(128)}, u32[]{:S(2)}) copy-start(f32[128]{0:T(128)} %param.17) | copy-start | bytes 1540
  7.4 88.3 %all-reduce.2.cloned.1.call-start = ((), (), s32[]{:S(2)}) async-start(), calls=%async_computation.1 | async-start | bytes 2097152 | tf_op jit(solution)/shard_map/psum | solution.py:133
  13.4 1.1 copy-start.3
  13.4 1.1 copy-start.6
  13.4 1.7 copy-start.2
  15.1 16.9 %copy-start.4 = (bf16[256,128]{1,0:T(8,128)(2,1)S(1)}, bf16[256,128]{1,0:T(8,128)(2,1)}, u32[]{:S(2)}) copy-start(bf16[256,128]{1,0:T(8,128)(2,1)} %param.16) | copy-start | bytes 196612
  48.4 2.2 copy-start.1
  53.0 2.2 copy-start.1
  58.0 109.6 %all-gather.4.cloned.1.call-start = ((), (), s32[]{:S(2)}) async-start(), calls=%async_computation.2 | async-start | bytes 7208960 | tf_op jit(solution)/shard_map/all_gather | solution.py:141
  58.6 215.4 %all-gather.6.cloned.1.call-start = ((), (), s32[]{:S(2)}) async-start(), calls=%async_computation.3 | async-start | bytes 7208960 | tf_op jit(solution)/shard_map/all_gather | solution.py:146
  59.2 321.0 %all-gather.8.cloned.1.call-start = ((), (), s32[]{:S(2)}) async-start(), calls=%async_computation.4 | async-start | bytes 7208960 | tf_op jit(solution)/shard_map/all_gather | solution.py:154
  59.8 107.8 %copy-start.8 = (f32[2048]{0:T(1024)S(1)}, f32[2048]{0:T(1024)}, u32[]{:S(2)}) copy-start(f32[2048]{0:T(1024)} %param.21) | copy-start | bytes 24580
  59.8 354.7 %reduce-scatter.2.cloned.1.call-start = ((), (), s32[]{:S(2)}) async-start(), calls=%async_computation.5 | async-start | bytes 1310720 | tf_op jit(solution)/shard_map/reduce_scatter | solution.py:155
  98.9 76.6 %copy-start.5 = (f32[3,1408]{1,0:T(4,128)S(1)}, f32[3,1408]{1,0:T(4,128)}, u32[]{:S(2)}) copy-start(f32[3,1408]{1,0:T(4,128)} %param.24) | copy-start | bytes 50692
  172.8 2.8 collective-permute-start
  174.1 5.5 %collective-permute-start.1 = (bf16[1,1408]{1,0:T(2,128)(2,1)S(1)}, bf16[1,1408]{1,0:T(2,128)(2,1)S(1)}, u32[]{:S(2)}, u32[]{:S(2)}) collective-permute-start(bf16[1,1408]{1,0:T(2,128)(2,1)S(1)} %get-tuple-element.117), channel_id=1, source_target_pairs={{4,0},{8,4},{12,8},{5,1},{9,5},{13,9},{6,2},{10,6},{14,10},{7,3},{... | collective-permute-start | bytes 8456 | tf_op jit(solution)/shard_map/ppermute | solution.py:20
Sparse Core Ops, SparseCore 0:
  58.1 37.4 all-reduce.1
  391.4 23.0 reduce-scatter.1
Sparse Core Ops, SparseCore 1:
  60.1 107.5 all-gather.3
  169.0 104.9 all-gather.5
  275.4 104.7 all-gather.7
where the time goes:
time: 424 us
  waiting for transfers between devices  333 us (79%)
  blocking collectives  30.2 us (7%)
  matrix products  22.8 us (5%)
  other arithmetic  16.5 us (4%)
  between operations  15.3 us (4%)
    all_gather x1, waiting for transfers between devices, local(): down_full = lax.all_gather(down_weight, 'sp', axis=1, tiled=True)  106 us
    all_gather x1, waiting for transfers between devices, local(): lax.all_gather(up_weight, 'sp', axis=0, tiled=True)  93.1 us
    all_gather x1, waiting for transfers between devices, local(): lax.all_gather(gate_weight, 'sp', axis=0, tiled=True)  68.7 us
    psum x1, waiting for transfers between devices, local(): lax.psum(jnp.dot(heads, out_weight, preferred_element_type=jnp.float32).a...  35.8 us
    reduce_scatter x1, waiting for transfers between devices, local(): lax.psum_scatter(jnp.dot(hidden, down_full, preferred_element_type=jnp.fl...  23.2 us
    all_gather x1, blocking collectives, local(): key_piece = lax.all_gather(key_flat, 'sp', axis=0, tiled=True)  15.7 us
    all_gather x1, blocking collectives, local(): value_piece = lax.all_gather(values, 'sp', axis=0, tiled=True)  14.6 us
    dot_general x1, matrix products, local(): jnp.dot(hidden, down_full, preferred_element_type=jnp.float32)  11.1 us
  transfers between devices with their start and end apart: 7, of which 6 were waited for; matrix products, arithmetic and copies ran while one was open for 2% of the time, Pallas kernels for 0%

commit v1 on v0

--- a/solution.py
+++ b/solution.py
@@ -151,7 +151,12 @@
     padded = padded_2(gate, (("sp", 0),), 1).astype(jnp.float32)
     conv = conv_taps[0] * padded[:-2] + conv_taps[1] * padded[1:-1] + conv_taps[2] * padded[2:]
     hidden = (jax.nn.silu(conv) * up_val.astype(jnp.float32)).astype(jnp.bfloat16)
-    down_full = lax.all_gather(down_weight, "sp", axis=1, tiled=True)
+    ring = [down_weight]
+    for hop in range(3):
+        ring.append(lax.ppermute(ring[-1], "sp", [(dev, (dev + 1) % 4) for dev in range(4)]))
+    down_full = jnp.roll(
+        jnp.concatenate(ring[::-1], axis=1), (lax.axis_index("sp") + 1) * ring[0].shape[1], axis=1
+    )
     mixer_out = lax.psum_scatter(
         jnp.dot(hidden, down_full, preferred_element_type=jnp.float32).astype(jnp.bfloat16),
         "tp",

time: 424 us -> 384 us (0.906)
  waiting for transfers between devices: 333 us -> 242 us
  starting transfers between devices: 2.93 us -> 32.3 us
  local copies, waits for them, and re-layouts: 3.61 us -> 22.2 us
    ppermute x0 -> x3, waiting for transfers between devices: none -> 159 us  [local(): lax.ppermute(ring[-1], 'sp', [(dev, (dev + 1) % 4) for dev in range(4)])]
    all_gather x1 -> x0, waiting for transfers between devices: 106 us -> none  [local(): down_full = lax.all_gather(down_weight, 'sp', axis=1, tiled=True)]
    all_gather x1, waiting for transfers between devices: 68.7 us -> 0.01 us  [local(): lax.all_gather(gate_weight, 'sp', axis=0, tiled=True)]
    psum x1, waiting for transfers between devices: 35.8 us -> 0.01 us  [local(): lax.psum(jnp.dot(heads, out_weight, preferred_element_type=jnp.float32).a...]
    all_gather x1, waiting for transfers between devices: 93.1 us -> 58.1 us  [local(): lax.all_gather(up_weight, 'sp', axis=0, tiled=True)]
    ppermute x0 -> x3, starting transfers between devices: none -> 26.2 us  [local(): lax.ppermute(ring[-1], 'sp', [(dev, (dev + 1) % 4) for dev in range(4)])]
    unnamed x16 -> x25, local copies, waits for them, and re-layouts: 0.04 us -> 16 us
  transfers between devices with their start and end apart: 7 -> 9, of which waited for: 6 -> 5; matrix products, arithmetic and copies ran while one was open for 2% -> 7% of each run, Pallas kernels for 0% -> 0%
where the time goes in v1:
time: 384 us; the launch traced here: 383 us
  waiting for transfers between devices  242 us (63%)
  starting transfers between devices  32.3 us (8%)
  blocking collectives  30.1 us (8%)
  matrix products  23.1 us (6%)
  local copies, waits for them, and re-layouts  22.2 us (6%)
  other arithmetic  18.9 us (5%)
  between operations  15.1 us (4%)
    ppermute x3, waiting for transfers between devices, local(): lax.ppermute(ring[-1], 'sp', [(dev, (dev + 1) % 4) for dev in range(4)])  159 us
    all_gather x1, waiting for transfers between devices, local(): lax.all_gather(up_weight, 'sp', axis=0, tiled=True)  58.1 us
    ppermute x3, starting transfers between devices, local(): lax.ppermute(ring[-1], 'sp', [(dev, (dev + 1) % 4) for dev in range(4)])  26.2 us
    reduce_scatter x1, waiting for transfers between devices, local(): lax.psum_scatter(jnp.dot(hidden, down_full, preferred_element_type=jnp.fl...  23.5 us
    unnamed x25, local copies, waits for them, and re-layouts  16 us
    all_gather x1, blocking collectives, local(): key_piece = lax.all_gather(key_flat, 'sp', axis=0, tiled=True)  15.7 us
    all_gather x1, blocking collectives, local(): value_piece = lax.all_gather(values, 'sp', axis=0, tiled=True)  14.4 us
    dot_general x1, matrix products, local(): jnp.dot(hidden, down_full, preferred_element_type=jnp.float32)  11.4 us
  transfers between devices with their start and end apart: 9, of which 5 were waited for; matrix products, arithmetic and copies ran while one was open for 7% of the time, Pallas kernels for 0%

profile of v1, /device:TPU:0, one launch (start us, length us, event | category | flops | bytes accessed | tf_op | source)
XLA Modules:
  0.0 383.4 jit_solution(6215482838377324401)
XLA Ops:
  7.4 0.0 all-reduce.2.cloned.1.call-start
  7.4 1.3 reshape.324
  8.7 1.9 reshape.323
  10.6 1.0 fusion.37
  11.6 0.9 fusion.39
  12.5 0.9 fusion.44
  13.5 0.1 broadcast_multiply_fusion.1
  13.6 1.7 fusion.42
  15.4 15.7 %all_gather.12 = bf16[1024,128]{1,0:T(8,128)(2,1)S(1)} all-gather(bf16[256,128]{1,0:T(8,128)(2,1)S(1)} %get-tuple-element.109), channel_id=1, replica_groups=mesh['grp'=2,'sp'=4,'tp'=4] {'sp'}, dimensions={0}, use_global_device_ids=true | all-gather | bytes 327680 | tf_op jit(solution)/shard_map/all_gather | solution.py:101
  31.0 0.3 multiply_reduce_fusion.2
  31.4 0.3 multiply_multiply_fusion
  31.8 0.9 fusion.33
  32.6 0.0 copy-start.7
  32.7 0.1 copy-done.5
  32.8 1.2 fusion.36
  34.0 14.4 %all_gather.13 = bf16[1024,128]{1,0:T(8,128)(2,1)S(1)} all-gather(bf16[256,128]{1,0:T(8,128)(2,1)S(1)} %copy-done.7), channel_id=1, replica_groups=mesh['grp'=2,'sp'=4,'tp'=4] {'sp'}, dimensions={0}, use_global_device_ids=true | all-gather | bytes 327680 | tf_op jit(solution)/shard_map/all_gather | solution.py:102
  48.4 9.3 %while.15 = (s32[]{:T(128)}, f32[1,1024]{1,0:T(1,128)S(1)}, f32[1,1024]{1,0:T(1,128)S(1)}, f32[1,1024,128]{2,1,0:T(8,128)S(1)}, bf16[2,512,1,128]{3,1,2,0:T(8,12...) while((s32[]{:T(128)}, f32[1,1024]{1,0:T(1,128)S(1)}, ...), condition=%wide.region_5.6_spmd.clone, body=%wide.region_2.5_spmd.clone.sunk | while | flops 273028096 | bytes 16318613 | solution.py:127
  48.4 1.8 multiply_reduce_fusion.4
  50.2 2.1 fusion.68
  52.4 0.1 copy-done.1
  52.4 0.6 fusion.70
  53.1 1.8 multiply_reduce_fusion.4
  54.9 2.1 fusion.68
  57.0 0.1 copy-done.1
  57.1 0.6 fusion.70
  57.7 0.2 divide_convert_fusion
  58.0 0.1 copy.27
  58.1 1.7 convolution_convert_fusion
  59.8 0.0 all-reduce.2.cloned.1.call-update
  59.9 0.0 all-gather.3.cloned.1.call-start
  59.9 0.5 all-gather.3.cloned.1.call-update
  60.5 0.0 all-gather.5.cloned.1.call-start
  60.5 0.5 all-gather.5.cloned.1.call-update
  61.0 0.0 reduce-scatter.2.cloned.1.call-start
  61.1 0.1 copy-done.2
  61.2 1.5 collective-permute-start.2
  62.7 51.8 %collective-permute-done.2 = bf16[1408,512]{1,0:T(8,128)(2,1)S(1)} collective-permute-done((bf16[1408,512]{1,0:T(8,128)(2,1)S(1)}, bf16[1408,512]{1,0:T(8,128)(2,1)S(1)}, u32[]{:S(2)}, u32[]{:S(2)}) %collective-permute-start.2) | collective-permute-done | bytes 1441824 | tf_op jit(solution)/shard_map/ppermute | solution.py:156
  114.5 1.1 copy-done.3
  115.6 14.2 %collective-permute-start.3 = (bf16[1408,512]{1,0:T(8,128)(2,1)S(1)}, bf16[1408,512]{1,0:T(8,128)(2,1)}, u32[]{:S(2)}, u32[]{:S(2)}) collective-permute-start(bf16[1408,512]{1,0:T(8,128)(2,1)S(1)} %collective-permute-done.2), channel_id=1, source_target_pairs={{0,4},{4,8},{8,12},{12,0},{1,5},{5,9},{9,13},{13,1},{2,6},{6,10},{... | collective-permute-start | bytes 4325384 | tf_op jit(solution)/shard_map/ppermute | solution.py:156
  129.8 69.7 %collective-permute-done.3 = bf16[1408,512]{1,0:T(8,128)(2,1)} collective-permute-done((bf16[1408,512]{1,0:T(8,128)(2,1)S(1)}, bf16[1408,512]{1,0:T(8,128)(2,1)}, u32[]{:S(2)}, u32[]{:S(2)}) %collective-permute-start.3) | collective-permute-done | bytes 1441824 | tf_op jit(solution)/shard_map/ppermute | solution.py:156
  199.5 10.4 %collective-permute-start.4 = (bf16[1408,512]{1,0:T(8,128)(2,1)}, bf16[1408,512]{1,0:T(8,128)(2,1)}, u32[]{:S(2)}, u32[]{:S(2)}) collective-permute-start(bf16[1408,512]{1,0:T(8,128)(2,1)} %collective-permute-done.3), channel_id=1, source_target_pairs={{0,4},{4,8},{8,12},{12,0},{1,5},{5,9},{9,13},{13,1},{2,6},{6,10},{... | collective-permute-start | bytes 4325384 | tf_op jit(solution)/shard_map/ppermute | solution.py:156
  210.0 1.5 slice_reduce_fusion.2
  211.5 3.2 convert_add_fusion
  214.7 0.5 add_rsqrt_fusion.1
  215.2 37.5 %collective-permute-done.4 = bf16[1408,512]{1,0:T(8,128)(2,1)} collective-permute-done((bf16[1408,512]{1,0:T(8,128)(2,1)}, bf16[1408,512]{1,0:T(8,128)(2,1)}, u32[]{:S(2)}, u32[]{:S(2)}) %collective-permute-start.4) | collective-permute-done | bytes 1441824 | tf_op jit(solution)/shard_map/ppermute | solution.py:156
  252.7 2.6 constant_dynamic-update-slice_fusion.7
  255.3 2.8 constant_dynamic-update-slice_fusion.6
  258.1 1.3 constant_dynamic-update-slice_fusion.5
  259.4 1.3 constant_dynamic-update-slice_fusion.4
  260.7 2.7 constant_dynamic-update-slice_fusion.3
  263.3 2.7 constant_dynamic-update-slice_fusion.2
  266.0 1.3 constant_dynamic-update-slice_fusion.1
  267.3 5.2 %convolution_convert_fusion.2 = bf16[256,1408]{1,0:T(8,128)(2,1)S(1)} fusion(bf16[2048,1408]{1,0:T(8,128)(2,1)} %all-gather.3.cloned.1.call-done, f32[2048]{0:T(1024)} %param.21, f32[256]{0:T(256)} %add_rsqrt_fusion.1, bf16[256,2048]{1,0:T(8,128)(2,1)} %all-reduce.2.cloned.1.call-done, bf16[256,2048]{1,0:T(8,128)(2,1)} %param.20), kind=kOutput, calls=%fused_computation.32 | convolution fusion | flops 1479901184 | bytes 8594432 | tf_op jit(solution)/shard_map/dot_general | solution.py:139
  272.5 1.3 collective-permute-start.1
  273.8 4.7 %collective-permute-start = (bf16[1,1408]{1,0:T(2,128)(2,1)S(1)}, bf16[1,1408]{1,0:T(2,128)(2,1)S(1)}, u32[]{:S(2)}, u32[]{:S(2)}) collective-permute-start(bf16[1,1408]{1,0:T(2,128)(2,1)S(1)} %get-tuple-element.116), channel_id=1, source_target_pairs={{0,4},{4,8},{8,12},{1,5},{5,9},{9,13},{2,6},{6,10},{10,14},{3,7},{... | collective-permute-start | bytes 8456 | tf_op jit(solution)/shard_map/ppermute | solution.py:17
  278.5 1.3 constant_dynamic-update-slice_fusion
  279.8 0.0 collective-permute-done.1
  279.8 0.0 collective-permute-done
  279.8 1.3 maximum_convert_fusion
  281.1 58.1 %all-gather.5.cloned.1.call-done = bf16[2048,1408]{1,0:T(8,128)(2,1)} async-done(((bf16[512,1408]{1,0:T(8,128)(2,1)}), bf16[2048,1408]{1,0:T(8,128)(2,1)}) %all-gather.5.cloned.1.call-update) | async-done | bytes 5767184 | tf_op jit(solution)/shard_map/all_gather | solution.py:146
  339.2 11.4 %fusion.20 = bf16[256,2048]{1,0:T(8,128)(2,1)} fusion(bf16[1408,4096]{1,0:T(8,128)(2,1)} %constant_dynamic-update-slice_fusion, s32[]{:T(128)S(6)} %select_n.39, bf16[2048,1408]{1,0:T(8,128)(2,1)} %all-gather.5.cloned.1.call-done, f32[258,1408]{1,0:T(8,128)} %maximum_convert_fusion, f32[1408]{0:T(1024)S(1)} %get-tuple-element.91, ...), kind=kOutput, calls=%fused_computation.27 | convolution fusion | flops 2961145856 | bytes 19034116 | tf_op jit(solution)/shard_map/dot_general | solution.py:161
  350.6 0.0 reduce-scatter.2.cloned.1.call-update
  350.6 23.5 %reduce-scatter.2.cloned.1.call-done = bf16[64,2048]{1,0:T(8,128)(2,1)} async-done(((bf16[256,2048]{1,0:T(8,128)(2,1)}), bf16[64,2048]{1,0:T(8,128)(2,1)}) %reduce-scatter.2.cloned.1.call-update) | async-done | bytes 262160 | tf_op jit(solution)/shard_map/reduce_scatter | solution.py:160
  374.1 1.9 add_convert_fusion
  (33 shorter events, 0.2 us)
Async XLA Ops:
  7.4 50.7 %copy-start = (bf16[512,2048]{1,0:T(8,128)(2,1)S(1)}, bf16[512,2048]{1,0:T(8,128)(2,1)}, u32[]{:S(2)}) copy-start(bf16[512,2048]{1,0:T(8,128)(2,1)} %param.19) | copy-start | bytes 6291460
  7.4 6.2 %copy-start.6 = (bf16[256,128]{1,0:T(8,128)(2,1)S(1)}, bf16[256,128]{1,0:T(8,128)(2,1)}, u32[]{:S(2)}) copy-start(bf16[256,128]{1,0:T(8,128)(2,1)} %param.15) | copy-start | bytes 196612
  7.4 6.2 %copy-start.8 = (f32[128]{0:T(128)S(1)}, f32[128]{0:T(128)}, u32[]{:S(2)}) copy-start(f32[128]{0:T(128)} %param.18) | copy-start | bytes 1540
  7.4 204.1 %all-reduce.2.cloned.1.call-start = ((), (), s32[]{:S(2)}) async-start(), calls=%async_computation.1 | async-start | bytes 2097152 | tf_op jit(solution)/shard_map/psum | solution.py:133
  10.6 20.8 %copy-start.9 = (f32[128]{0:T(128)S(1)}, f32[128]{0:T(128)}, u32[]{:S(2)}) copy-start(f32[128]{0:T(128)} %param.17) | copy-start | bytes 1540
  31.8 1.0 copy-start.5
  32.6 1.4 copy-start.7
  50.2 2.2 copy-start.1
  54.9 2.2 copy-start.1
  59.8 1.4 copy-start.2
  59.9 207.4 %all-gather.3.cloned.1.call-start = ((), (), s32[]{:S(2)}) async-start(), calls=%async_computation.2 | async-start | bytes 7208960 | tf_op jit(solution)/shard_map/all_gather | solution.py:141
  60.5 278.8 %all-gather.5.cloned.1.call-start = ((), (), s32[]{:S(2)}) async-start(), calls=%async_computation.3 | async-start | bytes 7208960 | tf_op jit(solution)/shard_map/all_gather | solution.py:146
  61.0 313.1 %reduce-scatter.2.cloned.1.call-start = ((), (), s32[]{:S(2)}) async-start(), calls=%async_computation.4 | async-start | bytes 1310720 | tf_op jit(solution)/shard_map/reduce_scatter | solution.py:160
  61.2 53.3 %collective-permute-start.2 = (bf16[1408,512]{1,0:T(8,128)(2,1)S(1)}, bf16[1408,512]{1,0:T(8,128)(2,1)S(1)}, u32[]{:S(2)}, u32[]{:S(2)}) collective-permute-start(bf16[1408,512]{1,0:T(8,128)(2,1)S(1)} %copy-done.2), channel_id=1, source_target_pairs={{0,4},{4,8},{8,12},{12,0},{1,5},{5,9},{9,13},{13,1},{2,6},{6,10},{... | collective-permute-start | bytes 4325384 | tf_op jit(solution)/shard_map/ppermute | solution.py:156
  114.5 1.1 copy-start.3
  115.6 83.9 %collective-permute-start.3 = (bf16[1408,512]{1,0:T(8,128)(2,1)S(1)}, bf16[1408,512]{1,0:T(8,128)(2,1)}, u32[]{:S(2)}, u32[]{:S(2)}) collective-permute-start(bf16[1408,512]{1,0:T(8,128)(2,1)S(1)} %collective-permute-done.2), channel_id=1, source_target_pairs={{0,4},{4,8},{8,12},{12,0},{1,5},{5,9},{9,13},{13,1},{2,6},{6,10},{... | collective-permute-start | bytes 4325384 | tf_op jit(solution)/shard_map/ppermute | solution.py:156
  199.5 53.2 %collective-permute-start.4 = (bf16[1408,512]{1,0:T(8,128)(2,1)}, bf16[1408,512]{1,0:T(8,128)(2,1)}, u32[]{:S(2)}, u32[]{:S(2)}) collective-permute-start(bf16[1408,512]{1,0:T(8,128)(2,1)} %collective-permute-done.3), channel_id=1, source_target_pairs={{0,4},{4,8},{8,12},{12,0},{1,5},{5,9},{9,13},{13,1},{2,6},{6,10},{... | collective-permute-start | bytes 4325384 | tf_op jit(solution)/shard_map/ppermute | solution.py:156
  255.3 2.8 copy-start.4
  272.5 7.3 %collective-permute-start.1 = (bf16[1,1408]{1,0:T(2,128)(2,1)S(1)}, bf16[1,1408]{1,0:T(2,128)(2,1)S(1)}, u32[]{:S(2)}, u32[]{:S(2)}) collective-permute-start(bf16[1,1408]{1,0:T(2,128)(2,1)S(1)} %get-tuple-element.117), channel_id=1, source_target_pairs={{4,0},{8,4},{12,8},{5,1},{9,5},{13,9},{6,2},{10,6},{14,10},{7,3},{... | collective-permute-start | bytes 8456 | tf_op jit(solution)/shard_map/ppermute | solution.py:20
  273.8 6.0 %collective-permute-start = (bf16[1,1408]{1,0:T(2,128)(2,1)S(1)}, bf16[1,1408]{1,0:T(2,128)(2,1)S(1)}, u32[]{:S(2)}, u32[]{:S(2)}) collective-permute-start(bf16[1,1408]{1,0:T(2,128)(2,1)S(1)} %get-tuple-element.116), channel_id=1, source_target_pairs={{0,4},{4,8},{8,12},{1,5},{5,9},{9,13},{2,6},{6,10},{10,14},{3,7},{... | collective-permute-start | bytes 8456 | tf_op jit(solution)/shard_map/ppermute | solution.py:17
Sparse Core Ops, SparseCore 0:
  60.0 37.5 all-reduce.1
  350.7 23.3 reduce-scatter.1
Sparse Core Ops, SparseCore 1:
  61.9 165.3 all-gather.2
  228.7 110.5 all-gather.4
